TPU v7x, 128 devices: a whole 4x4x4 slice. The times are simulated.
128 devices in a mesh: sp: 32 (over z, y, core), tp: 4 (over x).
Axes of the slice: x: 4, y: 4, z: 4, core: 2. Of those that a mesh axis runs over, the one named last changes fastest.
Arguments:
- layer_input: bfloat16 [32768, 2048], P('sp'), may hold values from -6 to 6
- query_weight: bfloat16 [2048, 1024], P(None, 'tp'), may hold values from -0.125 to 0.125
- key_weight: bfloat16 [2048, 1024], P(None, 'tp'), may hold values from -0.125 to 0.125
- value_weight: bfloat16 [2048, 1024], P(None, 'tp'), may hold values from -0.125 to 0.125
- outgate_weight: bfloat16 [2048, 1024], P(None, 'tp'), may hold values from -0.125 to 0.125
- ingate_weight: bfloat16 [2048, 8], replicated, may hold values from -12 to 12, as said below
- forget_weight: bfloat16 [2048, 8], replicated, may hold values from -0.125 to 0.125
- forget_bias: float32 [8], P('tp'), as said below
- forget_shift: float32 [256, 8], P('sp', 'tp'), may hold values from -1 to 1
- init_state: float32 [8, 128, 128], P('tp'), may hold values from -96 to 96
- head_gain: float32 [1024], P('tp'), may hold values from 0.1 to 1.9
- conv_gate_weight: bfloat16 [2048, 1024], P(None, 'tp'), may hold values from -0.125 to 0.125
- conv_input_weight: bfloat16 [2048, 1024], P(None, 'tp'), may hold values from -0.125 to 0.125
- conv_outgate_weight: bfloat16 [2048, 1024], P(None, 'tp'), may hold values from -0.125 to 0.125
- conv_taps: float32 [3, 1024], P(None, 'tp'), may hold values from -3.5 to 3.5
- memory_out_weight: bfloat16 [1024, 2048], replicated, may hold values from -0.125 to 0.125
- conv_out_weight: bfloat16 [1024, 2048], replicated, may hold values from -0.125 to 0.125
Outputs:
- mixed: bfloat16 [32768, 2048], P(('sp', 'tp'))
Inputs may be any that keep to these rules, and one draw needn't show every extreme that they name: `forget_bias`: every head's forget offset is at least 3. `ingate_weight`: the columns' scales may differ from head to head.
All inputs are finite; a program needn't handle non-finite values.
Results may differ from a plain program's by a relative error of at most 0.012.
The roundings to bfloat16 on the way count: a program that leaves them out, or rounds other values in their place, can miss the bound.
Values may be sent and summed in bfloat16 or wider, within the bound.
A program may use at most 128 MiB of HBM per device.

v0:
```python
import jax
import jax.numpy as jnp
from jax import lax
from jax.sharding import Mesh
from jax.sharding import PartitionSpec as P

BLOCK = 128
SP = ("sp_0", "sp_1", "sp_2")
SP_TP = ("sp_0", "sp_1", "sp_2", "tp")


norm_eps = 1e-05


def filled_with(shard, identity):
    return jax.tree.map(
        lambda part, zero: jnp.zeros_like(part) + jnp.asarray(zero, part.dtype), shard, identity
    )


def collected_together(shard, axis):
    leaves = jax.tree.leaves(shard)
    sequence = sorted(range(len(leaves)), key=lambda k: -leaves[k].size)
    width = (1, *leaves[sequence[0]].shape)[-1]
    lines = [
        jnp.pad(leaves[k].reshape(-1), (0, -leaves[k].size % width)).reshape(-1, width)
        for k in sequence
    ]
    both, at, found = (lax.all_gather(jnp.concatenate(lines), axis), 0, {})
    for k, line in zip(sequence, lines):
        slab = both[:, at : at + len(line)].reshape(len(both), -1)
        found[k] = slab[:, : leaves[k].size].reshape(-1, *leaves[k].shape)
        at += len(line)
    numbers = iter(range(len(leaves)))
    return jax.tree.map(lambda _: found[next(numbers)], shard)


def prefix_by_axis(shard, axes, combine, identity):
    before = start = filled_with(shard, identity)
    so_far = shard
    for axis in reversed(axes):
        peers, index = (lax.axis_size(axis), lax.axis_index(axis))
        pieces = collected_together(so_far, axis)
        inside, so_far = (start, start)
        for k in range(peers):
            passed = k < index
            so_far = combine(so_far, jax.tree.map(lambda part: part[k], pieces))
            inside = jax.tree.map(lambda new, old: jnp.where(passed, new, old), so_far, inside)
        before = combine(inside, before)
    return before


def passed_along(block, axis, distance):
    devices = range(lax.axis_size(axis))
    route = [(i - distance, i) for i in devices if i - distance in devices]
    return lax.ppermute(block, axis, route)


def merge_states(earlier, latter):
    earlier_state, earlier_max, earlier_decay = earlier
    latter_state, latter_max, latter_decay = latter
    joint_max = jnp.maximum(latter_decay + earlier_max, latter_max)
    joint_state = (
        jnp.exp(latter_decay + earlier_max - joint_max)[..., None, None] * earlier_state
        + jnp.exp(latter_max - joint_max)[..., None, None] * latter_state
    )
    return (joint_state, joint_max, earlier_decay + latter_decay)


def per_device(
    layer_input,
    query_weight,
    key_weight,
    value_weight,
    outgate_weight,
    ingate_weight,
    forget_weight,
    forget_bias,
    forget_shift,
    init_state,
    head_gain,
    conv_gate_weight,
    conv_input_weight,
    conv_outgate_weight,
    conv_taps,
    memory_out_weight,
    conv_out_weight,
):
    highest_value = lax.Precision.HIGHEST
    tokens = layer_input.shape[0]
    heads_here = init_state.shape[0]
    head_size = init_state.shape[1]
    blocks = tokens // BLOCK
    rescale_factor = head_size ** (-0.5)
    column = lax.axis_index("tp") * heads_here
    seq_index = lax.axis_index(SP)

    def stored(weight):
        return lax.optimization_barrier(
            jnp.dot(layer_input, weight, preferred_element_type=jnp.float32).astype(jnp.bfloat16)
        )

    query_proj = stored(query_weight)
    key_proj = stored(key_weight)
    value_proj = stored(value_weight)
    out_gate = stored(outgate_weight)
    gate_count = ingate_weight.shape[1]
    gate_logits = jnp.dot(
        layer_input,
        jnp.concatenate([ingate_weight, forget_weight], axis=1),
        preferred_element_type=jnp.float32,
    )
    in_gate = lax.dynamic_slice_in_dim(gate_logits, column, heads_here, 1).reshape(
        blocks, BLOCK, heads_here
    )
    forget_logits = lax.dynamic_slice_in_dim(
        gate_logits, gate_count + column, heads_here, 1
    ).reshape(blocks, BLOCK, heads_here)
    log_forget = jax.nn.log_sigmoid(
        forget_logits + forget_bias[None, None, :] + forget_shift[:, None, :]
    )
    cumulative = jnp.cumsum(log_forget, axis=1)
    block_decay = cumulative[:, -1]
    block_shape = (blocks, BLOCK, heads_here, head_size)
    query_blocks = query_proj.reshape(block_shape)
    key_blocks = key_proj.reshape(block_shape)
    value_blocks = value_proj.reshape(block_shape)
    end_logs = block_decay[:, None] - cumulative + in_gate
    local_max = end_logs.max(1)
    final_weights = jnp.exp(end_logs - local_max[:, None])
    state_within = jnp.einsum(
        "bshk,bshv->bhkv",
        key_blocks.astype(jnp.float32) * (rescale_factor * final_weights)[..., None],
        value_blocks.astype(jnp.float32),
        precision=highest_value,
    )
    neutral = (
        jnp.zeros((heads_here, head_size, head_size), jnp.float32),
        jnp.full((heads_here,), -1e30, jnp.float32),
        jnp.zeros((heads_here,), jnp.float32),
    )

    def advance(running, current):
        return (merge_states(running, current), running)

    summary, prefix = lax.scan(advance, neutral, (state_within, local_max, block_decay))
    dev_state, dev_max, dev_decay = summary
    at_front = seq_index == 0
    seeded = merge_states(
        (init_state, jnp.zeros((heads_here,), jnp.float32), jnp.zeros((heads_here,), jnp.float32)),
        summary,
    )
    element = (
        jnp.where(at_front, seeded[0], dev_state),
        jnp.where(at_front, seeded[1], dev_max),
        jnp.where(at_front, seeded[2], dev_decay),
    )
    scanned = prefix_by_axis(element, SP, merge_states, neutral)
    in_state = jnp.where(at_front, init_state, scanned[0])
    in_max = jnp.where(at_front, jnp.zeros((heads_here,), jnp.float32), scanned[1])
    entering = merge_states(
        (in_state[None], in_max[None], jnp.zeros((1, heads_here), jnp.float32)), prefix
    )
    enter_state = entering[0]
    enter_max = entering[1]
    decay_rows = jnp.swapaxes(cumulative, 1, 2)
    gate_rows = jnp.swapaxes(in_gate, 1, 2)
    causal = jnp.tril(jnp.ones((BLOCK, BLOCK), dtype=bool))
    pair_logs = jnp.where(
        causal[None, None],
        decay_rows[..., :, None] - decay_rows[..., None, :] + gate_rows[..., None, :],
        -1e30,
    )
    carry_log_values = decay_rows + enter_max[..., None]
    row_maximum = jnp.maximum(carry_log_values, pair_logs.max(-1))
    scores = jnp.einsum(
        "bjhd,bshd->bhjs", query_blocks, key_blocks, preferred_element_type=jnp.float32
    )
    weights = (scores * rescale_factor * jnp.exp(pair_logs - row_maximum[..., None])).astype(
        jnp.bfloat16
    )
    inner_part = jnp.einsum(
        "bhjs,bshv->bjhv", weights, value_blocks, preferred_element_type=jnp.float32
    )
    carried_over = jnp.einsum(
        "bjhk,bhkv->bjhv", query_blocks.astype(jnp.float32), enter_state, precision=highest_value
    )
    hidden = (
        inner_part
        + carried_over * jnp.swapaxes(jnp.exp(carry_log_values - row_maximum), 1, 2)[..., None]
    )
    hidden = hidden.reshape(tokens, heads_here, head_size)
    center = hidden.mean(-1, keepdims=True)
    spread = jnp.square(hidden - center).mean(-1, keepdims=True)
    normed = (
        (hidden - center) * lax.rsqrt(spread + norm_eps) * head_gain.reshape(heads_here, head_size)
    )
    memory_out = (
        jax.nn.sigmoid(out_gate.astype(jnp.float32))
        * normed.reshape(tokens, heads_here * head_size)
    ).astype(jnp.bfloat16)
    conv_gate = stored(conv_gate_weight)
    conv_input = stored(conv_input_weight)
    conv_outgate = stored(conv_outgate_weight)
    conv_in = conv_gate * conv_input
    lookback = conv_taps.shape[0] - 1
    edge_rows = passed_along(conv_in[tokens - lookback :], SP, 1)
    padded = jnp.concatenate([edge_rows, conv_in], axis=0)
    convolved = conv_taps[0][None, :] * padded[0:tokens].astype(jnp.float32)
    for offset in range(1, lookback + 1):
        convolved = convolved + conv_taps[offset][None, :] * padded[
            offset : offset + tokens
        ].astype(jnp.float32)
    conv_out = (conv_outgate.astype(jnp.float32) * convolved).astype(jnp.bfloat16)
    memory_rows, conv_rows = (
        lax.all_to_all(memory_out, "tp", split_axis=0, concat_axis=1, tiled=True),
        lax.all_to_all(conv_out, "tp", split_axis=0, concat_axis=1, tiled=True),
    )
    mixed = jnp.dot(memory_rows, memory_out_weight, preferred_element_type=jnp.float32) + jnp.dot(
        conv_rows, conv_out_weight, preferred_element_type=jnp.float32
    )
    return mixed.astype(jnp.bfloat16)


def solution(mesh):
    finer = Mesh(mesh.devices.reshape(4, 4, 2, mesh.shape["tp"]), ("sp_0", "sp_1", "sp_2", "tp"))
    in_specs = (
        P(SP, None),
        P(None, "tp"),
        P(None, "tp"),
        P(None, "tp"),
        P(None, "tp"),
        P(),
        P(),
        P("tp"),
        P(SP, "tp"),
        P("tp", None, None),
        P("tp"),
        P(None, "tp"),
        P(None, "tp"),
        P(None, "tp"),
        P(None, "tp"),
        P(),
        P(),
    )
    out_specs = P(SP_TP, None)
    return jax.shard_map(
        per_device, mesh=finer, in_specs=in_specs, out_specs=out_specs, check_vma=False
    )
```

profile of v0, /device:TPU:1, one launch (start us, length us, event | category | flops | bytes accessed | tf_op | source)
XLA Modules:
  0.0 145.8 jit_solution(13802680836486943526)
XLA Ops:
  0.1 3.5 %fusion.52 = f32[16,1024]{1,0:T(8,128)S(1)} fusion(bf16[1024,2048]{1,0:T(8,128)(2,1)} %param.19, bf16[2048,8]{0,1:T(8,128)(2,1)} %param.25, bf16[2048,8]{0,1:T(8,128)(2,1)} %param.24), kind=kOutput, calls=%fused_computation.92 | convolution fusion | flops 67239936 | bytes 4325376 | tf_op jit(solution)/shard_map/dot_general | solution.py:108
  3.6 0.6 dynamic-slice_bitcast_fusion.1
  4.6 23.3 %fusion.102 = f32[8,128,2]{2,0,1:T(8,128)S(1)} fusion(f32[8,128,2]{2,0,1:T(8,128)S(1)} %copy.98), kind=kOutput, calls=%fused_computation.255 | output fusion | flops 260096 | bytes 16384 | tf_op jit(solution)/shard_map/jit(cumsum)/reduce_window_sum | solution.py:122
  28.8 3.5 %convolution_convert_fusion.3 = bf16[1024,256]{1,0:T(8,128)(2,1)S(1)} fusion(bf16[1024,2048]{1,0:T(8,128)(2,1)} %param.19, bf16[2048,256]{1,0:T(8,128)(2,1)S(1)} %copy-done), kind=kOutput, calls=%fused_computation.28 | convolution fusion | flops 1074003968 | bytes 5767168 | tf_op jit(solution)/shard_map/dot_general | solution.py:100
  32.9 3.9 %convolution_convert_fusion.5 = bf16[1024,256]{1,0:T(8,128)(2,1)S(1)} fusion(bf16[1024,2048]{1,0:T(8,128)(2,1)} %param.19, bf16[2048,256]{1,0:T(8,128)(2,1)} %param.22), kind=kOutput, calls=%fused_computation.30 | convolution fusion | flops 1074003968 | bytes 5767168 | tf_op jit(solution)/shard_map/dot_general | solution.py:100
  36.9 1.1 copy.118
  38.0 2.2 %fusion.21 = f32[8,2,128,128]{3,2,1,0:T(8,128)S(1)} fusion(bf16[8,128,2,128]{1,3,2,0:T(8,128)(2,1)} %copy.118, bf16[8,128,2,128]{1,3,2,0:T(8,128)(2,1)S(1)} %copy.106, f32[8,128,2]{1,2,0:T(2,128)S(1)} %copy.107), kind=kOutput, calls=%fused_computation.44 | convolution fusion | flops 403177472 | bytes 2105344 | tf_op jit(solution)/shard_map/bshk,bshv->bhkv/dot_general | solution.py:131
  40.3 7.2 %while.21 = (s32[]{:T(128)}, f32[2,128,128]{2,1,0:T(8,128)S(1)}, f32[2]{0:T(128)S(1)}, f32[2]{0:T(128)S(1)}, f32[8,2,128,128]{3,2,1,0:T(8,128)}, /*index=5*/f32[...) while((s32[]{:T(128)}, f32[2,128,128]{2,1,0:T(8,128)S(1)}, ...), condition=%wide.region_3.4_spmd.clone, body=%wide.region_2.3_spmd.clone.sunk | while | flops 163859 | bytes 656174 | solution.py:146
  40.3 0.7 bitcast_dynamic-update-slice_fusion.2
  41.2 0.7 bitcast_dynamic-update-slice_fusion.2
  42.1 0.7 bitcast_dynamic-update-slice_fusion.2
  43.0 0.7 bitcast_dynamic-update-slice_fusion.2
  44.0 0.7 bitcast_dynamic-update-slice_fusion.2
  44.9 0.7 bitcast_dynamic-update-slice_fusion.2
  45.8 0.7 bitcast_dynamic-update-slice_fusion.2
  46.7 0.7 bitcast_dynamic-update-slice_fusion.2
  47.7 3.0 %all-gather.3 = f32[2,258,128]{2,1,0:T(8,128)S(1)} all-gather(f32[1,258,128]{2,1,0:T(8,128)S(1)} %maximum_bitcast_fusion), channel_id=2, replica_groups=mesh['sp_0'=4,'sp_1'=4,'sp_2'=2,'tp'=4] {'sp_2'}, dimensions={0}, use_global_device_ids=true | all-gather | bytes 396288 | tf_op jit(solution)/shard_map/all_gather | solution.py:29
  51.3 11.6 %all-gather.4 = f32[4,258,128]{2,1,0:T(8,128)S(1)} all-gather(f32[1,258,128]{2,1,0:T(8,128)S(1)} %maximum_bitcast_fusion.1), channel_id=3, replica_groups=mesh['sp_0'=4,'sp_1'=4,'sp_2'=2,'tp'=4] {'sp_1'}, dimensions={0}, use_global_device_ids=true | all-gather | bytes 660480 | tf_op jit(solution)/shard_map/all_gather | solution.py:29
  64.0 11.4 %all-gather.5 = f32[4,258,128]{2,1,0:T(8,128)S(1)} all-gather(f32[1,258,128]{2,1,0:T(8,128)S(1)} %maximum_bitcast_fusion.2), channel_id=4, replica_groups=mesh['sp_0'=4,'sp_1'=4,'sp_2'=2,'tp'=4] {'sp_0'}, dimensions={0}, use_global_device_ids=true | all-gather | bytes 660480 | tf_op jit(solution)/shard_map/all_gather | solution.py:29
  75.4 0.8 fusion.92
  76.3 0.8 fusion.93
  78.4 0.7 copy.115
  79.0 0.8 copy.99
  79.8 0.6 fusion.60
  80.7 0.7 fusion.24
  81.8 0.8 copy.122
  82.6 3.7 %convolution_convert_fusion.4 = bf16[1024,256]{1,0:T(8,128)(2,1)S(1)} fusion(bf16[1024,2048]{1,0:T(8,128)(2,1)} %param.19, bf16[2048,256]{1,0:T(8,128)(2,1)} %param.20), kind=kOutput, calls=%fused_computation.29 | convolution fusion | flops 1074003968 | bytes 5767168 | tf_op jit(solution)/shard_map/dot_general | solution.py:100
  86.5 1.0 fusion.59
  88.2 0.9 subtract_exponential_fusion.9
  89.0 0.7 fusion.61
  89.7 1.7 %add_select_fusion.2 = f32[2,128,128]{2,1,0:T(8,128)S(1)} fusion(f32[2,128,128]{2,1,0:T(8,128)S(1)} %copy-done.6, f32[2,128,128]{2,1,0:T(8,128)S(1)} %bitcast.421, f32[2,128,128]{2,1,0:T(8,128)S(1)} %bitcast.420, f32[2,128,128]{2,1,0:T(8,128)} %bitcast.430, f32[2,128,128]{2,1,0:T(8,128)} %bitcast.429, f32[2,128,128]{2,1,0:T(8,128)} %bitcast.428, ...), kind=kLoop, calls=%fused_computation.90 | loop fusion | flops 1507328 | bytes 1573083 | tf_op jit(solution)/shard_map/jit(_where)/select_n | solution.py:159
  91.5 3.3 %fusion.11 = f32[8,128,2,128]{1,3,2,0:T(8,128)} fusion(f32[8,2,128,128]{3,2,1,0:T(8,128)} %get-tuple-element.67, f32[8,128,2]{1,2,0:T(2,128)} %copy.122, f32[8,2]{1,0:T(8,128)} %subtract_exponential_fusion.2, f32[2,128,128]{2,1,0:T(8,128)S(1)} %add_select_fusion.2, f32[8,2]{1,0:T(8,128)} %get-tuple-element.163, bf16[8,128,2,128]{3,2,1,0:T(2,128)(2,1)S(1)} %reshape.874), kind=kOutput, calls=%fused_computation.23 | convolution fusion | flops 403701760 | bytes 2760832 | tf_op jit(solution)/shard_map/bjhk,bhkv->bjhv/dot_general | solution.py:185
  94.8 2.3 %fusion.99 = (f32[8,128,2]{1,2,0:T(2,128)S(1)}, f32[8,128,2,128]{1,3,2,0:T(8,128)S(1)}) fusion(f32[8,128,2,128]{1,3,2,0:T(8,128)} %fusion.11, bf16[8,128,2,128]{1,3,2,0:T(8,128)(2,1)S(1)} %copy-done.4, bf16[8,128,2,128]{1,3,2,0:T(8,128)(2,1)S(1)} %copy-done.3, f32[8,2,128]{2,1,0:T(2,128)} %copy.117, f32[8,2,128]{2,1,0:T(2,128)S(1)} %copy-done.11, ...), kind=kOutput, calls=%fused_computation.254 | convolution fusion | flops 136574976 | bytes 3719168 | tf_op jit(solution)/shard_map/bhjs,bshv->bjhv/dot_general | solution.py:182
  97.1 0.6 copy.123
  98.4 3.7 %convolution_convert_fusion.6 = bf16[1024,256]{1,0:T(8,128)(2,1)S(1)} fusion(bf16[1024,2048]{1,0:T(8,128)(2,1)} %param.19, bf16[2048,256]{1,0:T(8,128)(2,1)} %param.23), kind=kOutput, calls=%fused_computation.31 | convolution fusion | flops 1074003968 | bytes 5767168 | tf_op jit(solution)/shard_map/dot_general | solution.py:100
  102.1 1.2 mul.589
  103.3 1.2 sub.312
  105.0 1.0 copy.126
  106.0 4.1 %all-to-all-start = ((bf16[4,256,256]{1,2,0:T(8,128)(2,1)}), bf16[4,256,256]{1,2,0:T(8,128)(2,1)S(1)}, u32[]{:S(2)}, u32[]{:S(2)}) async-start(bf16[4,256,256]{1,2,0:T(8,128)(2,1)} %copy.126), calls=%async_computation | async-start | bytes 1048576 | tf_op jit(solution)/shard_map/all_to_all | solution.py:216
  110.1 3.9 %convolution_convert_fusion.1 = bf16[1024,256]{1,0:T(8,128)(2,1)S(1)} fusion(bf16[1024,2048]{1,0:T(8,128)(2,1)} %param.19, bf16[2048,256]{1,0:T(8,128)(2,1)} %param.30), kind=kOutput, calls=%fused_computation.26 | convolution fusion | flops 1074003968 | bytes 5767168 | tf_op jit(solution)/shard_map/dot_general | solution.py:100
  114.0 1.3 convolution_convert_fusion
  115.4 9.3 %collective-permute-start = (bf16[2,256]{1,0:T(2,128)(2,1)S(1)}, bf16[2,256]{1,0:T(2,128)(2,1)S(1)}, u32[]{:S(2)}, u32[]{:S(2)}) collective-permute-start(bf16[2,256]{1,0:T(2,128)(2,1)S(1)} %slice.238), channel_id=1, source_target_pairs={{0,4},{4,8},{8,12},{12,16},{16,20},{20,24},{24,28},{28,32},{32,36}... | collective-permute-start | bytes 3080 | tf_op jit(solution)/shard_map/ppermute | solution.py:56
  124.7 1.3 convolution_convert_fusion.2
  126.5 1.0 copy.127
  127.5 4.5 %all-to-all-start.1 = ((bf16[4,256,256]{1,2,0:T(8,128)(2,1)}), bf16[4,256,256]{1,2,0:T(8,128)(2,1)S(1)}, u32[]{:S(2)}, u32[]{:S(2)}) async-start(bf16[4,256,256]{1,2,0:T(8,128)(2,1)} %copy.127), calls=%async_computation.1 | async-start | bytes 1048576 | tf_op jit(solution)/shard_map/all_to_all | solution.py:217
  132.0 4.8 %fusion.103 = f32[256,2048]{1,0:T(8,128)} fusion(bf16[256,1024]{0,1:T(8,128)(2,1)S(1)} %bitcast.418, bf16[1024,2048]{1,0:T(8,128)(2,1)} %param.34), kind=kOutput, calls=%fused_computation.256 | convolution fusion | flops 1073741824 | bytes 6815744 | tf_op jit(solution)/shard_map/dot_general | solution.py:219
  136.8 3.8 %all-to-all-done.1 = bf16[4,256,256]{1,2,0:T(8,128)(2,1)S(1)} async-done(((bf16[4,256,256]{1,2,0:T(8,128)(2,1)}), bf16[4,256,256]{1,2,0:T(8,128)(2,1)S(1)}, u32[]{:S(2)}, u32[]{:S(2)}) %all-to-all-start.1) | async-done | bytes 524320 | tf_op jit(solution)/shard_map/all_to_all | solution.py:217
  140.7 5.1 %fusion.8 = bf16[256,2048]{1,0:T(8,128)(2,1)} fusion(f32[256,2048]{1,0:T(8,128)} %fusion.103, bf16[256,1024]{0,1:T(8,128)(2,1)S(1)} %bitcast.419, bf16[1024,2048]{1,0:T(8,128)(2,1)} %param.35), kind=kOutput, calls=%fused_computation.17 | convolution fusion | flops 1074790400 | bytes 7864320 | tf_op jit(solution)/shard_map/dot_general | solution.py:219
  (181 shorter events, 9.4 us)
Async XLA Ops:
  0.0 28.8 %copy-start = (bf16[2048,256]{1,0:T(8,128)(2,1)S(1)}, bf16[2048,256]{1,0:T(8,128)(2,1)}, u32[]{:S(2)}) copy-start(bf16[2048,256]{1,0:T(8,128)(2,1)} %param.21) | copy-start | bytes 3145732
  0.0 4.2 %copy-start.27 = (f32[2]{0:T(128)S(1)}, f32[2]{0:T(128)}, u32[]{:S(2)}) copy-start(f32[2]{0:T(128)} %param.26) | copy-start | bytes 28
  0.0 4.2 %copy-start.26 = (f32[8,2]{0,1:T(2,128)S(1)}, f32[8,2]{0,1:T(2,128)}, u32[]{:S(2)}) copy-start(f32[8,2]{0,1:T(2,128)} %param.27) | copy-start | bytes 196
  32.8 5.2 %copy-start.2 = (bf16[8,128,2,128]{1,3,2,0:T(8,128)(2,1)}, bf16[8,128,2,128]{1,3,2,0:T(8,128)(2,1)S(1)}, u32[]{:S(2)}) copy-start(bf16[8,128,2,128]{1,3,2,0:T(8,128)(2,1)S(1)} %copy.106) | copy-start | bytes 1572868
  36.8 10.8 %copy-start.6 = (f32[2,128,128]{2,1,0:T(8,128)S(1)}, f32[2,128,128]{2,1,0:T(8,128)}, u32[]{:S(2)}) copy-start(f32[2,128,128]{2,1,0:T(8,128)} %param.28) | copy-start | bytes 393220
  47.5 33.2 %copy-start.10 = (f32[8,2,128]{2,1,0:T(2,128)S(1)}, f32[8,2,128]{2,1,0:T(2,128)}, u32[]{:S(2)}) copy-start(f32[8,2,128]{2,1,0:T(2,128)} %get-tuple-element.200) | copy-start | bytes 24580
  50.7 0.6 copy-start.13
  50.7 12.2 %copy-start.21 = (f32[2]{0:T(128)}, f32[2]{0:T(128)S(1)}, u32[]{:S(2)}) copy-start(f32[2]{0:T(128)S(1)} %get-tuple-element.232) | copy-start | bytes 28
  50.7 12.2 %copy-start.22 = (f32[2]{0:T(128)}, f32[2]{0:T(128)S(1)}, u32[]{:S(2)}) copy-start(f32[2]{0:T(128)S(1)} %get-tuple-element.233) | copy-start | bytes 28
  50.9 12.1 %copy-start.23 = (f32[2]{0:T(128)}, f32[2]{0:T(128)S(1)}, u32[]{:S(2)}) copy-start(f32[2]{0:T(128)S(1)} %get-tuple-element.231) | copy-start | bytes 28
  62.9 13.3 %copy-start.24 = (f32[2]{0:T(128)}, f32[2]{0:T(128)S(1)}, u32[]{:S(2)}) copy-start(f32[2]{0:T(128)S(1)} %get-tuple-element.174) | copy-start | bytes 28
  63.0 1.0 copy-start.14
  63.0 1.0 copy-start.15
  63.0 13.2 %copy-start.16 = (f32[2]{0:T(128)}, f32[2]{0:T(128)S(1)}, u32[]{:S(2)}) copy-start(f32[2]{0:T(128)S(1)} %get-tuple-element.222) | copy-start | bytes 28
  63.0 13.2 %copy-start.17 = (f32[2]{0:T(128)}, f32[2]{0:T(128)S(1)}, u32[]{:S(2)}) copy-start(f32[2]{0:T(128)S(1)} %get-tuple-element.223) | copy-start | bytes 28
  63.1 13.2 %copy-start.18 = (f32[2]{0:T(128)}, f32[2]{0:T(128)S(1)}, u32[]{:S(2)}) copy-start(f32[2]{0:T(128)S(1)} %get-tuple-element.225) | copy-start | bytes 28
  63.1 13.2 %copy-start.19 = (f32[2]{0:T(128)}, f32[2]{0:T(128)S(1)}, u32[]{:S(2)}) copy-start(f32[2]{0:T(128)S(1)} %get-tuple-element.226) | copy-start | bytes 28
  63.1 13.2 %copy-start.20 = (f32[2]{0:T(128)}, f32[2]{0:T(128)S(1)}, u32[]{:S(2)}) copy-start(f32[2]{0:T(128)S(1)} %get-tuple-element.227) | copy-start | bytes 28
  75.4 6.3 %copy-start.8 = (f32[4,1,128]{2,1,0:T(1,128)}, f32[4,1,128]{2,1,0:T(1,128)S(1)}, u32[]{:S(2)}) copy-start(f32[4,1,128]{2,1,0:T(1,128)S(1)} %get-tuple-element.192) | copy-start | bytes 6148
  75.4 6.3 %copy-start.9 = (f32[4,1,128]{2,1,0:T(1,128)}, f32[4,1,128]{2,1,0:T(1,128)S(1)}, u32[]{:S(2)}) copy-start(f32[4,1,128]{2,1,0:T(1,128)S(1)} %get-tuple-element.193) | copy-start | bytes 6148
  77.1 4.7 %copy-start.7 = (pred[128,128]{1,0:T(8,128)(4,1)}, pred[128,128]{1,0:T(8,128)(4,1)S(1)}, u32[]{:S(2)}) copy-start(pred[128,128]{1,0:T(8,128)(4,1)S(1)} %iota_compare_fusion) | copy-start | bytes 49156
  86.4 8.4 %copy-start.3 = (bf16[8,128,2,128]{1,3,2,0:T(8,128)(2,1)S(1)}, bf16[8,128,2,128]{1,3,2,0:T(8,128)(2,1)}, u32[]{:S(2)}) copy-start(bf16[8,128,2,128]{1,3,2,0:T(8,128)(2,1)} %copy-done.2) | copy-start | bytes 1572868
  86.4 8.4 %copy-start.4 = (bf16[8,128,2,128]{1,3,2,0:T(8,128)(2,1)S(1)}, bf16[8,128,2,128]{1,3,2,0:T(8,128)(2,1)}, u32[]{:S(2)}) copy-start(bf16[8,128,2,128]{1,3,2,0:T(8,128)(2,1)} %copy.118) | copy-start | bytes 1572868
  86.5 4.9 %copy-start.5 = (bf16[8,128,2,128]{3,2,1,0:T(2,128)(2,1)}, bf16[8,128,2,128]{3,2,1,0:T(2,128)(2,1)S(1)}, u32[]{:S(2)}) copy-start(bf16[8,128,2,128]{3,2,1,0:T(2,128)(2,1)S(1)} %reshape.874) | copy-start | bytes 1572868
  87.6 7.2 %copy-start.11 = (f32[8,2,128]{2,1,0:T(2,128)S(1)}, f32[8,2,128]{2,1,0:T(2,128)}, u32[]{:S(2)}) copy-start(f32[8,2,128]{2,1,0:T(2,128)} %get-tuple-element.200) | copy-start | bytes 24580
  98.3 6.2 %copy-start.25 = (f32[256]{0:T(256)S(1)}, f32[256]{0:T(256)}, u32[]{:S(2)}) copy-start(f32[256]{0:T(256)} %param.29) | copy-start | bytes 3076
  106.0 8.0 %copy-start.28 = (bf16[2048,256]{1,0:T(8,128)(2,1)S(1)}, bf16[2048,256]{1,0:T(8,128)(2,1)}, u32[]{:S(2)}) copy-start(bf16[2048,256]{1,0:T(8,128)(2,1)} %param.31) | copy-start | bytes 3145732
  106.0 21.5 %all-to-all-start = ((bf16[4,256,256]{1,2,0:T(8,128)(2,1)}), bf16[4,256,256]{1,2,0:T(8,128)(2,1)S(1)}, u32[]{:S(2)}, u32[]{:S(2)}) async-start(bf16[4,256,256]{1,2,0:T(8,128)(2,1)} %copy.126), calls=%async_computation | async-start | bytes 1048576 | tf_op jit(solution)/shard_map/all_to_all | solution.py:216
  110.1 3.9 %copy-start.1 = (bf16[1024,2048]{1,0:T(8,128)(2,1)S(1)}, bf16[1024,2048]{1,0:T(8,128)(2,1)}, u32[]{:S(2)}) copy-start(bf16[1024,2048]{1,0:T(8,128)(2,1)} %param.19) | copy-start | bytes 12582916
  114.0 10.7 %copy-start.29 = (bf16[2048,256]{1,0:T(8,128)(2,1)S(1)}, bf16[2048,256]{1,0:T(8,128)(2,1)}, u32[]{:S(2)}) copy-start(bf16[2048,256]{1,0:T(8,128)(2,1)} %param.32) | copy-start | bytes 3145732
  115.3 10.7 %copy-start.12 = (f32[3,256]{1,0:T(4,128)S(1)}, f32[3,256]{1,0:T(4,128)}, u32[]{:S(2)}) copy-start(f32[3,256]{1,0:T(4,128)} %param.33) | copy-start | bytes 9220
  115.4 10.6 %collective-permute-start = (bf16[2,256]{1,0:T(2,128)(2,1)S(1)}, bf16[2,256]{1,0:T(2,128)(2,1)S(1)}, u32[]{:S(2)}, u32[]{:S(2)}) collective-permute-start(bf16[2,256]{1,0:T(2,128)(2,1)S(1)} %slice.238), channel_id=1, source_target_pairs={{0,4},{4,8},{8,12},{12,16},{16,20},{20,24},{24,28},{28,32},{32,36}... | collective-permute-start | bytes 3080 | tf_op jit(solution)/shard_map/ppermute | solution.py:56
  127.5 13.2 %all-to-all-start.1 = ((bf16[4,256,256]{1,2,0:T(8,128)(2,1)}), bf16[4,256,256]{1,2,0:T(8,128)(2,1)S(1)}, u32[]{:S(2)}, u32[]{:S(2)}) async-start(bf16[4,256,256]{1,2,0:T(8,128)(2,1)} %copy.127), calls=%async_computation.1 | async-start | bytes 1048576 | tf_op jit(solution)/shard_map/all_to_all | solution.py:217
where the time goes:
time: 146 us
  matrix products  42.5 us (29%)
  other arithmetic  38.9 us (27%)
  blocking collectives  26 us (18%)
  starting transfers between devices  17.9 us (12%)
  local copies, waits for them, and re-layouts  15.6 us (11%)
  waiting for transfers between devices  3.83 us (3%)
    all_gather x3, blocking collectives, collected_together(): both, at, found = (lax.all_gather(jnp.concatenate(lines), axis), 0, {})  26 us
    another operation x1, other arithmetic, per_device(): cumulative = jnp.cumsum(log_forget, axis=1)  23.3 us
    dot_general x7, matrix products, stored(): jnp.dot(layer_input, weight, preferred_element_type=jnp.float32)  21.2 us
    ppermute x1, starting transfers between devices, passed_along(): return lax.ppermute(block, axis, route)  9.28 us
    dynamic_update_slice x8, other arithmetic, per_device(): lax.scan(advance, neutral, (state_within, local_max, block_decay))  5.37 us
    dot_general x1, matrix products, per_device(): jnp.dot(conv_rows, conv_out_weight, preferred_element_type=jnp.float32)  5.11 us
    dot_general x1, matrix products, per_device(): jnp.dot(memory_rows, memory_out_weight, preferred_element_type=jnp.float32)  4.82 us
    all_to_all x1, starting transfers between devices, per_device(): lax.all_to_all(conv_out, 'tp', split_axis=0, concat_axis=1, tiled=True)  4.51 us
  transfers between devices with their start and end apart: 3, of which 1 were waited for; matrix products, arithmetic and copies ran while one was open for 9% of the time, Pallas kernels for 0%

commit v1 on v0

v1 whole, which is shorter than its diff:
```python
import functools

import jax
import jax.numpy as jnp
from jax import lax
from jax.experimental import pallas as pl
from jax.experimental.pallas import tpu as pltpu
from jax.sharding import Mesh
from jax.sharding import PartitionSpec as P

F32, BF16 = jnp.float32, jnp.bfloat16
MESH = pl.DeviceIdType.MESH
BLOCK = 128
EPS = 1e-05
LOW = -1e30
TAIL = 16
AXES = ("z", "y", "c", "tp")


def mm(a, b):
    return jnp.dot(a, b, preferred_element_type=F32)


def mm_nt(a, b):
    return lax.dot_general(a, b, (((1,), (1,)), ((), ())), preferred_element_type=F32)


def merge(earlier, latter):
    e_s, e_m, e_d = earlier
    l_s, l_m, l_d = latter
    top = jnp.maximum(l_d + e_m, l_m)
    return jnp.exp(l_d + e_m - top) * e_s + jnp.exp(l_m - top) * l_s, top, e_d + l_d


def pick(cond, a, b):
    return tuple(jnp.where(cond, u, v) for u, v in zip(a, b))


def thirds(v):
    hi = v.astype(BF16).astype(F32)
    mid = (v - hi).astype(BF16).astype(F32)
    return hi, mid, v - hi - mid


def pack(ref, triple):
    s, m, d = triple
    dk, lanes = s.shape
    row = lax.broadcasted_iota(jnp.int32, (TAIL, lanes), 0)
    tail = jnp.zeros((TAIL, lanes), F32)
    for k, part in enumerate((*thirds(m), *thirds(d))):
        tail = jnp.where(row == k, part, tail)
    ref[0:dk, :] = s.astype(BF16)
    ref[dk : dk + TAIL, :] = tail.astype(BF16)


def unpack(ref):
    dk = ref.shape[0] - TAIL
    tail = ref[dk : dk + TAIL, :].astype(F32)
    m = tail[0:1] + tail[1:2] + tail[2:3]
    d = tail[3:4] + tail[4:5] + tail[5:6]
    return ref[0:dk, :].astype(F32), m, d


def kernel(sizes, *refs):
    nz, ny, nc, nt = sizes
    (x_hbm, wk_hbm, wv_hbm, wcg_hbm, wci_hbm, wco_hbm, wq_hbm, wog_hbm, wi_hbm, wf_hbm,
     fb, fs, init_hbm, gain_hbm, taps_hbm, wmo_hbm, wcout_hbm, out_v) = refs[:18]
    (x_v, w_v, wi_v, wf_v, init_v, gain_v, taps_v, wmo_v, wcout_v,
     k_v, v_v, q_v, co_v, og_v, cin_v, hloc_v, acc_v,
     gt_v, rows_v, col_v, fac_v, vt_v, pref_v, bd_v,
     edge_v, halo_v, msg_v, ry_v, msgr_v, rz_v, zs_v, zmd_v, msg4_v, r4_v, ah_v, ahmd_v,
     csend_v, crow_v, msend_v, mrow_v,
     ld_sem, one_send, one_recv, y_send, y_recv, z_send, z_recv,
     c_send, c_recv, m_send, m_recv) = refs[18:]

    z, y, c, t = (lax.axis_index(a) for a in AXES)
    n_sp = nz * ny * nc
    sp = (z * ny + y) * nc + c

    def at_sp(index):
        return {"z": lax.div(index, ny * nc), "y": lax.rem(lax.div(index, nc), ny), "c": lax.rem(index, nc)}

    after = at_sp(lax.rem(sp + 1, n_sp))
    before = at_sp(lax.rem(sp + n_sp - 1, n_sp))
    tokens = x_v.shape[0]
    part = tokens // nt
    nb = tokens // BLOCK
    width = k_v.shape[1]
    heads = width // BLOCK
    dh = BLOCK
    scale = dh ** -0.5
    per = part // BLOCK
    near = sorted(range(1, nt), key=lambda d: -min(d, nt - d))
    plane = [(dy, dc) for dy in (*sorted(range(1, ny), key=lambda d: -min(d, ny - d)), 0) for dc in range(nc) if dy or dc]

    def chunk(r):
        return pl.ds(r * part, part)

    loads = {}

    def load(name, src, dst):
        copy = pltpu.make_async_copy(src, dst, ld_sem.at[len(loads)])
        copy.start()
        loads[name] = copy

    def need(*names):
        for name in names:
            loads[name].wait()

    load("x0", x_hbm.at[chunk(0)], x_v.at[chunk(0)])
    load("k", wk_hbm, w_v.at[0])
    load("wi", wi_hbm, wi_v)
    load("wf", wf_hbm, wf_v)
    for r in range(1, nt):
        load("x%d" % r, x_hbm.at[chunk(r)], x_v.at[chunk(r)])
    load("v", wv_hbm, w_v.at[1])

    bar = pltpu.get_barrier_semaphore()

    def greet(device):
        pl.semaphore_signal(bar, inc=1, device_id=device, device_id_type=MESH)

    def turn(dy, dc):
        return {"y": lax.rem(y + dy, ny), "c": lax.rem(c + dc, nc)}

    for d in range(1, nt):
        greet({"tp": lax.rem(t + d, nt)})
    for dy, dc in plane:
        greet(turn(dy, dc))
    greet(before)
    for zz in range(nz - 1):

        @pl.when(zz < z)
        def _():
            greet({"z": zz})

    def remote(src, dst, send, recv, device):
        return pltpu.make_async_remote_copy(
            src_ref=src, dst_ref=dst, send_sem=send, recv_sem=recv, device_id=device, device_id_type=MESH
        )

    need("wi", "wf")
    wg_t = jnp.concatenate([wi_v[...].astype(F32), wf_v[...].astype(F32)], axis=0).astype(BF16)
    for r in range(nt):
        need("x%d" % r)
        if r == 0:
            need("k")
        if r == 1:
            load("cg", wcg_hbm, w_v.at[2])
            load("ci", wci_hbm, w_v.at[3])
            load("init", init_hbm, init_v)
        xr = x_v[chunk(r), :]
        logits = mm_nt(wg_t, xr)
        for b in range(part // BLOCK):
            gt_v[r * (part // BLOCK) + b] = logits[:, b * BLOCK : (b + 1) * BLOCK]
        k_v[chunk(r), :] = mm(xr, w_v[0]).astype(BF16)
    need("v", "init", "cg", "ci")
    load("taps", taps_hbm, taps_v)
    load("co", wco_hbm, w_v.at[4])
    load("q", wq_hbm, w_v.at[5])
    load("og", wog_hbm, w_v.at[6])
    load("gain", gain_hbm, gain_v)
    load("cout", wcout_hbm, wcout_v)
    load("mo", wmo_hbm, wmo_v)

    def conv_input(xr):
        gate = mm(xr, w_v[2]).astype(BF16)
        inp = mm(xr, w_v[3]).astype(BF16)
        return (gate.astype(F32) * inp.astype(F32)).astype(BF16).astype(F32)

    edge_v[...] = conv_input(x_v[tokens - 16 : tokens, :])

    n_gate = gt_v.shape[1] // 2
    n_row = heads * nb
    for h in range(heads):
        for b in range(nb):
            row = h * nb + b
            rows_v[0, row : row + 1, :] = gt_v[b, pl.ds(t * heads + h, 1), :]
            rows_v[1, row : row + 1, :] = gt_v[b, pl.ds(n_gate + t * heads + h, 1), :] + fb[h] + fs[h, b]
    shape = (n_row, BLOCK)
    lane = lax.broadcasted_iota(jnp.int32, shape, 1)
    in_gate = rows_v[0]
    logit = rows_v[1]
    cum = jnp.minimum(logit, 0.0) - jnp.log1p(jnp.exp(-jnp.abs(logit)))
    step = 1
    while step < BLOCK:
        cum = cum + jnp.where(lane >= step, pltpu.roll(cum, step, 1), 0.0)
        step *= 2
    lead = in_gate - cum
    high = lead
    step = 1
    while step < BLOCK:
        high = jnp.maximum(high, jnp.where(lane >= step, pltpu.roll(high, step, 1), LOW))
        step *= 2
    decay = jnp.broadcast_to(cum[:, BLOCK - 1 : BLOCK], shape)
    end_log = decay - cum + in_gate
    loc_max = jnp.broadcast_to(jnp.max(end_log, axis=1, keepdims=True), shape)
    final = jnp.exp(end_log - loc_max) * scale
    rows_v[0] = decay
    rows_v[1] = loc_max
    rows_v[2] = final
    rows_v[5] = lead
    for r in range(nt):
        v_v[chunk(r), :] = mm(x_v[chunk(r), :], w_v[1]).astype(BF16)

    first = sp == 0
    states = []
    for h in range(heads):
        top = jnp.where(first, jnp.zeros((1, BLOCK), F32), jnp.full((1, BLOCK), LOW, F32))
        state = jnp.where(first, init_v[h].T, jnp.zeros((dh, dh), F32))
        states.append((state, top, jnp.zeros((1, BLOCK), F32)))
    for b in range(nb):
        rows = slice(b * BLOCK, (b + 1) * BLOCK)
        for h in range(heads):
            head = slice(h * dh, (h + 1) * dh)
            row = h * nb + b
            state, top, past = states[h]
            pref_v[row] = state.astype(BF16)
            rows_v[3, row : row + 1, :] = top
            rows_v[4, row : row + 1, :] = past
            value_t = v_v[rows, head].astype(F32).T
            vt_v[row] = value_t.astype(BF16)
            within = mm((value_t * rows_v[2, row : row + 1, :]).astype(BF16), k_v[rows, head])
            states[h] = merge(states[h], (within, rows_v[1, row : row + 1, :], rows_v[0, row : row + 1, :]))
    for h in range(heads):
        pack(msg_v.at[h], states[h])

    spot = y * nc + c
    pl.semaphore_wait(bar, (nt - 1) + len(plane) + 1 + (nz - 1 - z))
    halo = remote(edge_v.at[pl.ds(8, 8)], halo_v, one_send.at[0], one_recv.at[0], after)
    halo.start()
    started = [halo]
    for i, (dy, dc) in enumerate(plane):
        to = turn(dy, dc)
        copy = remote(msg_v.at[to["c"]], ry_v.at[spot], y_send.at[i], y_recv.at[spot], to)
        copy.start()
        started.append(copy)
    ry_v[pl.ds(spot, 1)] = msg_v[pl.ds(c, 1)]

    local_top = rows_v[3]
    peak = jnp.maximum(local_top, high)
    rows_v[6] = peak
    rows_v[7] = jnp.exp(local_top - peak)
    col_v[0:n_row, :] = rows_v[5]
    col_v[...] = col_v[...].T

    for r in range(nt):
        cin_v[pl.ds(8 + r * part, part), :] = conv_input(x_v[chunk(r), :])
    need("taps", "co", "q")
    mine_lanes = pl.ds(pl.multiple_of(t * width, width), width)
    order = (*range(1, nt), 0)

    def outgate_query(r):
        xr = x_v[chunk(r), :]
        q_v[chunk(r), :] = mm(xr, w_v[5]).astype(BF16)
        co_v[chunk(r), :] = mm(xr, w_v[4]).astype(BF16)

    outgate_query(order[0])
    for i, r in enumerate(order):
        if i + 1 < nt:
            outgate_query(order[i + 1])
        if r == 0:
            halo.wait_recv()
            cin_v[0:8, :] = jnp.where(first, jnp.zeros((8, width), F32), halo_v[...])
        strip = 64
        for k in range(0, part, strip):
            at = r * part + k
            window = cin_v[at : at + strip + 8, :]
            conv = taps_v[0:1, :] * window[6 : strip + 6]
            conv = conv + taps_v[1:2, :] * window[7 : strip + 7]
            conv = conv + taps_v[2:3, :] * window[8 : strip + 8]
            csend_v[r, k : k + strip, :] = (co_v[at : at + strip, :].astype(F32) * conv).astype(BF16)

        @pl.when(r != t)
        def _():
            remote(csend_v.at[r], crow_v.at[:, mine_lanes], c_send.at[r], c_recv.at[t], {"tp": r}).start()

    need("og", "gain")

    def output_gate(r):
        gate = jax.nn.sigmoid(mm(x_v[chunk(r), :], w_v[6]).astype(BF16).astype(F32)) * gain_v[0:1, :]
        for i in range(per):
            for h in range(heads):
                og_v[h, r * per + i] = gate[i * BLOCK : (i + 1) * BLOCK, h * dh : (h + 1) * dh].T

    output_gate(0)
    output_gate(1)

    for i, (dy, dc) in enumerate(plane):
        far = turn(dy, dc)
        slot = far["y"] * nc + far["c"]
        remote(msg_v.at[c], ry_v.at[slot], y_send.at[i], y_recv.at[slot], far).wait_recv()
    neutral = (jnp.zeros((dh, dh), F32), jnp.full((1, BLOCK), LOW, F32), jnp.zeros((1, BLOCK), F32))
    run = ahead = partner = neutral
    for i in range(ny * nc):
        run = merge(run, unpack(ry_v.at[i]))
        if i < ny * nc - 1:
            ahead = pick(i < spot, run, ahead)
            partner = pick(i < y * nc + 1 - c, run, partner)
    pack(msgr_v, run)
    for dz in sorted(range(1, nz), key=lambda d: -min(d, nz - d)):
        zz = z + dz

        @pl.when(zz < nz)
        def _():
            remote(msgr_v, rz_v.at[z], z_send.at[dz], z_recv.at[z], {"z": zz}).start()

    for k, triple in enumerate((ahead, partner)):
        ah_v[k] = triple[0]
        ahmd_v[k, 0:1, :] = triple[1]
        ahmd_v[k, 1:2, :] = triple[2]

    for r in range(2, nt):
        output_gate(r)

    causal = lax.broadcasted_iota(jnp.int32, (BLOCK, BLOCK), 0) <= lax.broadcasted_iota(jnp.int32, (BLOCK, BLOCK), 1)
    for b in range(nb):
        rows = slice(b * BLOCK, (b + 1) * BLOCK)
        for h in range(heads):
            head = slice(h * dh, (h + 1) * dh)
            row = h * nb + b
            query = q_v[rows, head]
            score = mm_nt(k_v[rows, head], query)
            logs = jnp.where(causal, col_v[:, row : row + 1] - rows_v[6, row : row + 1, :], LOW)
            weight = (score * scale * jnp.exp(logs)).astype(BF16)
            hidden = mm(vt_v[row], weight) + rows_v[7, row : row + 1, :] * mm_nt(pref_v[row], query)
            hloc_v[h, b] = hidden - jnp.mean(hidden, axis=0, keepdims=True)

    zs_v[...] = neutral[0]
    zmd_v[0:1, :] = neutral[1]
    zmd_v[1:2, :] = neutral[2]
    for zz in range(nz - 1):

        @pl.when(zz < z)
        def _():
            remote(msgr_v, rz_v.at[zz], z_send.at[0], z_recv.at[zz], {"z": zz}).wait_recv()
            zs, zm, zd = merge((zs_v[...], zmd_v[0:1, :], zmd_v[1:2, :]), unpack(rz_v.at[zz]))
            zs_v[...] = zs
            zmd_v[0:1, :] = zm
            zmd_v[1:2, :] = zd

    rows_before = (zs_v[...], zmd_v[0:1, :], zmd_v[1:2, :])
    pack(msg4_v, merge(rows_before, (ah_v[1], ahmd_v[1, 0:1, :], ahmd_v[1, 1:2, :])))
    give = remote(msg4_v, r4_v, one_send.at[1], one_recv.at[1], {"c": 1 - c})
    give.start()
    started.append(give)
    entering = merge(rows_before, (ah_v[0], ahmd_v[0, 0:1, :], ahmd_v[0, 1:2, :]))

    def prepare(k, g, triple):
        state, top, _ = triple
        bd_v[k] = (state - jnp.mean(state, axis=0, keepdims=True)).astype(BF16)
        rows = pl.ds(pl.multiple_of(g * nb, nb), nb)
        peak = rows_v[6, rows, :]
        carry = rows_v[4, rows, :] + top
        joint = jnp.maximum(peak, carry)
        fac_v[k, 0] = jnp.exp(peak - joint)
        fac_v[k, 1] = jnp.exp(carry - joint)

    def output(k, g, d):
        r = lax.rem(t + d, nt)
        rows = pl.ds(pl.multiple_of(r * part, part), part)
        head = pl.ds(pl.multiple_of(g * dh, dh), dh)
        carried = mm_nt(bd_v[k], q_v[rows, head])
        for i in range(per):
            b = r * per + i
            hidden = fac_v[k, 0, pl.ds(b, 1), :] * hloc_v[g, b]
            hidden = hidden + fac_v[k, 1, pl.ds(b, 1), :] * carried[:, i * BLOCK : (i + 1) * BLOCK]
            spread = jnp.mean(hidden * hidden, axis=0, keepdims=True)
            out = og_v[g, b] * (hidden * lax.rsqrt(spread + EPS))
            msend_v[d, g, i * BLOCK : (i + 1) * BLOCK, :] = out.T.astype(BF16)
        if d:
            copy = remote(msend_v.at[d, g], mrow_v.at[t, g], m_send.at[d, g], m_recv.at[t, g], {"tp": r})
            copy.start()
            started.append(copy)

    prepare(0, c, entering)
    for d in near:
        output(0, c, d)
    give.wait_recv()
    prepare(1, 1 - c, unpack(r4_v))
    for d in near:
        output(1, 1 - c, d)
    output(0, c, 0)
    output(1, 1 - c, 0)

    need("cout", "mo")
    for d in near:
        r = lax.rem(t + d, nt)
        lanes = pl.ds(pl.multiple_of(r * width, width), width)
        remote(csend_v.at[r], crow_v.at[:, lanes], c_send.at[r], c_recv.at[r], {"tp": r}).wait_recv()
    crow_v[:, mine_lanes] = csend_v[t]
    tile = min(512, acc_v.shape[1])
    tiles = [slice(n * tile, (n + 1) * tile) for n in range(acc_v.shape[1] // tile)]

    def weight_rows(r):
        return pl.ds(pl.multiple_of(r * width, width), width)

    def both(ref, k):
        return jnp.concatenate([ref[k, h] for h in range(heads)], axis=1)

    for cols in tiles:
        acc_v[:, cols] = mm(crow_v[...], wcout_v[:, cols]) + mm(both(msend_v, 0), wmo_v[weight_rows(t), cols])
    for k, d in enumerate(near):
        r = lax.rem(t + d, nt)
        for h in range(heads):
            remote(msend_v.at[d, h], mrow_v.at[r, h], m_send.at[d, h], m_recv.at[r, h], {"tp": r}).wait_recv()
        for cols in tiles:
            total = acc_v[:, cols] + mm(both(mrow_v, r), wmo_v[weight_rows(r), cols])
            if k == len(near) - 1:
                out_v[:, cols] = total.astype(BF16)
            else:
                acc_v[:, cols] = total

    for copy in started:
        copy.wait_send()
    for r in range(nt):

        @pl.when(r != t)
        def _():
            remote(csend_v.at[r], crow_v.at[:, mine_lanes], c_send.at[r], c_recv.at[t], {"tp": r}).wait_send()

    for dz in range(1, nz):
        zz = z + dz

        @pl.when(zz < nz)
        def _():
            remote(msgr_v, rz_v.at[z], z_send.at[dz], z_recv.at[z], {"z": zz}).wait_send()


def per_device(sizes, layer_input, query_weight, key_weight, value_weight, outgate_weight, ingate_weight,
               forget_weight, forget_bias, forget_shift, init_state, head_gain, conv_gate_weight,
               conv_input_weight, conv_outgate_weight, conv_taps, memory_out_weight, conv_out_weight):
    nz, ny, nc, nt = sizes
    tokens, model = layer_input.shape
    width = query_weight.shape[1]
    heads, dh, _ = init_state.shape
    gates = ingate_weight.shape[1]
    nb = tokens // BLOCK
    part = tokens // nt
    channels = memory_out_weight.shape[0]
    out_width = memory_out_weight.shape[1]
    n_row = heads * nb
    dma = pltpu.SemaphoreType.DMA
    vm = pltpu.VMEM
    msg = (dh + TAIL, dh)
    scratch = [
        vm((tokens, model), BF16), vm((7, model, width), BF16), vm((gates, model), BF16), vm((gates, model), BF16),
        vm((heads, dh, dh), F32), vm((1, width), F32), vm(conv_taps.shape, F32),
        vm((channels, out_width), BF16), vm((channels, out_width), BF16),
        vm((tokens, width), BF16), vm((tokens, width), BF16), vm((tokens, width), BF16), vm((tokens, width), BF16),
        vm((heads, nb, dh, BLOCK), F32), vm((tokens + 8, width), F32), vm((heads, nb, dh, BLOCK), F32),
        vm((part, out_width), F32),
        vm((nb, 2 * gates, BLOCK), F32), vm((8, n_row, BLOCK), F32), vm((BLOCK, BLOCK), F32),
        vm((heads, 2, nb, BLOCK), F32), vm((n_row, dh, dh), BF16), vm((n_row, dh, dh), BF16), vm((heads, dh, dh), BF16),
        vm((16, width), F32), vm((8, width), F32), vm((heads, *msg), BF16), vm((ny * nc, *msg), BF16), vm(msg, BF16),
        vm((nz, *msg), BF16), vm((dh, dh), F32), vm((8, dh), F32), vm(msg, BF16), vm(msg, BF16),
        vm((heads, dh, dh), F32), vm((heads, 8, dh), F32),
        vm((nt, part, width), BF16), vm((part, channels), BF16),
        vm((nt, heads, part, dh), BF16), vm((nt, heads, part, dh), BF16),
        dma((24,)), dma((2,)), dma((2,)), dma((ny * nc,)), dma((ny * nc,)), dma((nz,)), dma((nz,)),
        dma((nt,)), dma((nt,)), dma((nt, heads)), dma((nt, heads)),
    ]
    anywhere = pl.BlockSpec(memory_space=pltpu.HBM)
    smem = pl.BlockSpec(memory_space=pltpu.SMEM)
    return pl.pallas_call(
        functools.partial(kernel, sizes),
        out_shape=pltpu.VMEM((part, out_width), BF16),
        in_specs=[anywhere] * 10 + [smem] * 2 + [anywhere] * 5,
        out_specs=pl.BlockSpec(memory_space=pltpu.VMEM),
        scratch_shapes=scratch,
        compiler_params=pltpu.CompilerParams(
            collective_id=0, has_side_effects=True, vmem_limit_bytes=65994752
        ),
    )(layer_input, key_weight, value_weight, conv_gate_weight, conv_input_weight, conv_outgate_weight,
      query_weight, outgate_weight, ingate_weight.T, forget_weight.T, forget_bias, forget_shift.T, init_state,
      head_gain.reshape(1, -1), conv_taps, memory_out_weight, conv_out_weight)


def build(mesh, sizes):
    finer = Mesh(mesh.devices.reshape(sizes), AXES)
    sp = AXES[:3]
    in_specs = (
        P(sp, None), P(None, "tp"), P(None, "tp"), P(None, "tp"), P(None, "tp"), P(), P(), P("tp"), P(sp, "tp"),
        P("tp", None, None), P("tp"), P(None, "tp"), P(None, "tp"), P(None, "tp"), P(None, "tp"), P(), P(),
    )
    return jax.shard_map(
        functools.partial(per_device, sizes), mesh=finer, in_specs=in_specs, out_specs=P(AXES, None), check_vma=False
    )


def solution(mesh):
    return build(mesh, (4, 4, 2, mesh.shape["tp"]))
```

time: 146 us -> 30.4 us (0.21)
  matrix products: 42.5 us -> 0 us
  other arithmetic: 38.9 us -> 0 us
  Pallas kernels: 0 us -> 29.3 us
  blocking collectives: 26 us -> 0 us
  starting transfers between devices: 17.9 us -> 0 us
  local copies, waits for them, and re-layouts: 15.6 us -> 0.97 us
  waiting for transfers between devices: 3.83 us -> 0 us
    dot_general x13 -> x0, matrix products: 42.5 us -> none  [the longest x7 21.2 us: stored(): jnp.dot(layer_input, weight, preferred_element_type=jnp.float32)]
    pallas_call x0 -> x1, Pallas kernels: none -> 29.3 us  [per_device(): pl.pallas_call(functools.partial(kernel, sizes), out_shape=pltpu.VMEM((pa...]
    all_gather x3 -> x0, blocking collectives: 26 us -> none  [collected_together(): both, at, found = (lax.all_gather(jnp.concatenate(lines), axis), 0, {})]
    another operation x3 -> x0, other arithmetic: 23.3 us -> none  [the longest x1 23.3 us: per_device(): cumulative = jnp.cumsum(log_forget, axis=1)]
    ppermute x1 -> x0, starting transfers between devices: 9.28 us -> none  [passed_along(): return lax.ppermute(block, axis, route)]
    all_to_all x2 -> x0, starting transfers between devices: 8.59 us -> none  [the longest x1 4.51 us: per_device(): lax.all_to_all(conv_out, 'tp', split_axis=0, concat_axis=1, tiled=True)]
    dynamic_update_slice x8 -> x0, other arithmetic: 5.37 us -> none  [per_device(): lax.scan(advance, neutral, (state_within, local_max, block_decay))]
    all_to_all x2 -> x0, waiting for transfers between devices: 3.83 us -> none  [the longest x1 3.82 us: per_device(): lax.all_to_all(conv_out, 'tp', split_axis=0, concat_axis=1, tiled=True)]
  transfers between devices with their start and end apart: 3 -> 0, of which waited for: 1 -> 0; matrix products, arithmetic and copies ran while one was open for 9% -> 0% of each run, Pallas kernels for 0% -> 0%
where the time goes in v1:
time: 30.4 us; the launch traced here: 30.3 us
  Pallas kernels  29.3 us (96%)
  local copies, waits for them, and re-layouts  0.97 us (3%)
    pallas_call x1, Pallas kernels, per_device(): pl.pallas_call(functools.partial(kernel, sizes), out_shape=pltpu.VMEM((pa...  29.3 us
    unnamed x1, local copies, waits for them, and re-layouts  0.97 us

profile of v1, /device:TPU:1, one launch (start us, length us, event | category | flops | bytes accessed | tf_op | source)
XLA Modules:
  0.0 30.3 jit_solution(12128856313994363553)
XLA Ops:
  0.0 29.3 %shard_map.163 = bf16[256,2048]{1,0:T(8,128)(2,1)S(1)} custom-call(bf16[1024,2048]{1,0:T(8,128)(2,1)} %refs_0_.1, bf16[2048,256]{1,0:T(8,128)(2,1)} %refs_1_.1, bf16[2048,256]{1,0:T(8,128)(2,1)} %refs_2_.1, bf16[2048,256]{1,0:T(8,128)(2,1)} %refs_3_.1, bf16[2048,256]{1,0:T(8,128)(2,1)} %refs_4_.1, bf16[2048,256]{1,0:T(8,128)(2,1)} %refs_5_.1, ...), custom_call_target="tpu_custom_call" | custom-call | tf_op jit(solution)/shard_map/pallas_call | solution.py:465
  29.3 1.0 %copy.19 = bf16[256,2048]{1,0:T(8,128)(2,1)} copy(bf16[256,2048]{1,0:T(8,128)(2,1)S(1)} %shard_map.163) | data formatting | bytes 2097152

commit v2 on v1

--- a/solution.py
+++ b/solution.py
@@ -71,7 +71,7 @@
      edge_v, halo_v, msg_v, ry_v, msgr_v, rz_v, zs_v, zmd_v, msg4_v, r4_v, ah_v, ahmd_v,
      csend_v, crow_v, msend_v, mrow_v,
      ld_sem, one_send, one_recv, y_send, y_recv, z_send, z_recv,
-     c_send, c_recv, m_send, m_recv) = refs[18:]
+     c_send, c_recv, e_send, e_recv, m_send, m_recv) = refs[18:]
 
     z, y, c, t = (lax.axis_index(a) for a in AXES)
     n_sp = nz * ny * nc
@@ -248,32 +248,46 @@
         cin_v[pl.ds(8 + r * part, part), :] = conv_input(x_v[chunk(r), :])
     need("taps", "co", "q")
     mine_lanes = pl.ds(pl.multiple_of(t * width, width), width)
-    order = (*range(1, nt), 0)
+    order = [lax.rem(t + d, nt) for d in (*near, 0)]
+    cin_v[0:8, :] = jnp.zeros((8, width), F32)
 
     def outgate_query(r):
-        xr = x_v[chunk(r), :]
-        q_v[chunk(r), :] = mm(xr, w_v[5]).astype(BF16)
-        co_v[chunk(r), :] = mm(xr, w_v[4]).astype(BF16)
+        rows = pl.ds(pl.multiple_of(r * part, part), part)
+        xr = x_v[rows, :]
+        q_v[rows, :] = mm(xr, w_v[5]).astype(BF16)
+        co_v[rows, :] = mm(xr, w_v[4]).astype(BF16)
+
+    def convolve(at, n):
+        window = cin_v[pl.ds(at, n + 8), :]
+        conv = taps_v[0:1, :] * window[6 : n + 6]
+        conv = conv + taps_v[1:2, :] * window[7 : n + 7]
+        conv = conv + taps_v[2:3, :] * window[8 : n + 8]
+        return (co_v[pl.ds(at, n), :].astype(F32) * conv).astype(BF16)
+
+    def conv_copy(r, source, rows, recv):
+        lanes = pl.ds(pl.multiple_of(source * width, width), width)
+        return remote(csend_v.at[r, rows], crow_v.at[rows, lanes], c_send.at[r], recv, {"tp": r})
+
+    whole = pl.ds(0, part)
+    later = pl.ds(16, part - 16)
+    early = pl.ds(0, 16)
 
     outgate_query(order[0])
     for i, r in enumerate(order):
         if i + 1 < nt:
             outgate_query(order[i + 1])
-        if r == 0:
-            halo.wait_recv()
-            cin_v[0:8, :] = jnp.where(first, jnp.zeros((8, width), F32), halo_v[...])
         strip = 64
         for k in range(0, part, strip):
-            at = r * part + k
-            window = cin_v[at : at + strip + 8, :]
-            conv = taps_v[0:1, :] * window[6 : strip + 6]
-            conv = conv + taps_v[1:2, :] * window[7 : strip + 7]
-            conv = conv + taps_v[2:3, :] * window[8 : strip + 8]
-            csend_v[r, k : k + strip, :] = (co_v[at : at + strip, :].astype(F32) * conv).astype(BF16)
-
-        @pl.when(r != t)
-        def _():
-            remote(csend_v.at[r], crow_v.at[:, mine_lanes], c_send.at[r], c_recv.at[t], {"tp": r}).start()
+            csend_v[r, k : k + strip, :] = convolve(pl.multiple_of(r * part + k, strip), strip)
+        if i + 1 < nt:
+
+            @pl.when(r != 0)
+            def _():
+                conv_copy(r, t, whole, c_recv.at[t]).start()
+
+            @pl.when(r == 0)
+            def _():
+                conv_copy(r, t, later, c_recv.at[t]).start()
 
     need("og", "gain")
 
@@ -309,6 +323,18 @@
         ah_v[k] = triple[0]
         ahmd_v[k, 0:1, :] = triple[1]
         ahmd_v[k, 1:2, :] = triple[2]
+
+    halo.wait_recv()
+    cin_v[0:8, :] = jnp.where(first, jnp.zeros((8, width), F32), halo_v[...])
+    csend_v[0, 0:16, :] = convolve(0, 16)
+
+    def edge_copy(source):
+        lanes = pl.ds(pl.multiple_of(source * width, width), width)
+        return remote(csend_v.at[0, early], crow_v.at[early, lanes], e_send.at[0], e_recv.at[source], {"tp": 0})
+
+    @pl.when(t != 0)
+    def _():
+        edge_copy(t).start()
 
     for r in range(2, nt):
         output_gate(r)
@@ -376,18 +402,26 @@
     prepare(0, c, entering)
     for d in near:
         output(0, c, d)
+    output(0, c, 0)
     give.wait_recv()
     prepare(1, 1 - c, unpack(r4_v))
     for d in near:
         output(1, 1 - c, d)
-    output(0, c, 0)
     output(1, 1 - c, 0)
 
     need("cout", "mo")
     for d in near:
         r = lax.rem(t + d, nt)
-        lanes = pl.ds(pl.multiple_of(r * width, width), width)
-        remote(csend_v.at[r], crow_v.at[:, lanes], c_send.at[r], c_recv.at[r], {"tp": r}).wait_recv()
+
+        @pl.when(t != 0)
+        def _():
+            conv_copy(0, r, whole, c_recv.at[r]).wait_recv()
+
+        @pl.when(t == 0)
+        def _():
+            conv_copy(0, r, later, c_recv.at[r]).wait_recv()
+            edge_copy(r).wait_recv()
+
     crow_v[:, mine_lanes] = csend_v[t]
     tile = min(512, acc_v.shape[1])
     tiles = [slice(n * tile, (n + 1) * tile) for n in range(acc_v.shape[1] // tile)]
@@ -413,11 +447,16 @@
 
     for copy in started:
         copy.wait_send()
-    for r in range(nt):
-
-        @pl.when(r != t)
-        def _():
-            remote(csend_v.at[r], crow_v.at[:, mine_lanes], c_send.at[r], c_recv.at[t], {"tp": r}).wait_send()
+    for r in order[:-1]:
+
+        @pl.when(r != 0)
+        def _():
+            conv_copy(r, t, whole, c_recv.at[t]).wait_send()
+
+        @pl.when(r == 0)
+        def _():
+            conv_copy(r, t, later, c_recv.at[t]).wait_send()
+            edge_copy(t).wait_send()
 
     for dz in range(1, nz):
         zz = z + dz
@@ -458,7 +497,7 @@
         vm((nt, part, width), BF16), vm((part, channels), BF16),
         vm((nt, heads, part, dh), BF16), vm((nt, heads, part, dh), BF16),
         dma((24,)), dma((2,)), dma((2,)), dma((ny * nc,)), dma((ny * nc,)), dma((nz,)), dma((nz,)),
-        dma((nt,)), dma((nt,)), dma((nt, heads)), dma((nt, heads)),
+        dma((nt,)), dma((nt,)), dma((1,)), dma((nt,)), dma((nt, heads)), dma((nt, heads)),
     ]
     anywhere = pl.BlockSpec(memory_space=pltpu.HBM)
     smem = pl.BlockSpec(memory_space=pltpu.SMEM)

time: 30.4 us -> 29.8 us (0.980)
  Pallas kernels: 29.3 us -> 28.7 us
    pallas_call x1, Pallas kernels: 29.3 us -> 28.7 us  [per_device(): pl.pallas_call(functools.partial(kernel, sizes), out_shape=pltpu.VMEM((pa...]
where the time goes in v2:
time: 29.8 us; the launch traced here: 29.7 us
  Pallas kernels  28.7 us (96%)
  local copies, waits for them, and re-layouts  0.97 us (3%)
    pallas_call x1, Pallas kernels, per_device(): pl.pallas_call(functools.partial(kernel, sizes), out_shape=pltpu.VMEM((pa...  28.7 us
    unnamed x1, local copies, waits for them, and re-layouts  0.97 us

profile of v2, /device:TPU:1, one launch (start us, length us, event | category | flops | bytes accessed | tf_op | source)
XLA Modules:
  0.0 29.7 jit_solution(11435612631770210913)
XLA Ops:
  0.0 28.7 %shard_map.163 = bf16[256,2048]{1,0:T(8,128)(2,1)S(1)} custom-call(bf16[1024,2048]{1,0:T(8,128)(2,1)} %refs_0_.1, bf16[2048,256]{1,0:T(8,128)(2,1)} %refs_1_.1, bf16[2048,256]{1,0:T(8,128)(2,1)} %refs_2_.1, bf16[2048,256]{1,0:T(8,128)(2,1)} %refs_3_.1, bf16[2048,256]{1,0:T(8,128)(2,1)} %refs_4_.1, bf16[2048,256]{1,0:T(8,128)(2,1)} %refs_5_.1, ...), custom_call_target="tpu_custom_call" | custom-call | tf_op jit(solution)/shard_map/pallas_call | solution.py:504
  28.7 1.0 %copy.19 = bf16[256,2048]{1,0:T(8,128)(2,1)} copy(bf16[256,2048]{1,0:T(8,128)(2,1)S(1)} %shard_map.163) | data formatting | bytes 2097152
